TPU v7x, 256 devices: a 4x2x16 block of a 4x16x16 slice. The times are simulated.
256 devices in a mesh: grp: 2 (over y), sp: 32 (over z, core), tp: 4 (over x).
Axes of the slice: x: 4, y: 2, z: 16, core: 2. Of those that a mesh axis runs over, the one named last changes fastest.
The devices are a block of a 4x16x16 slice.
Arguments:
- ssm_input: bfloat16 [8192, 1024], P(('grp', 'sp'), 'tp'), parts along dimension 0, may hold values from -6 to 6
- residual_in: bfloat16 [8192, 2048], P(('grp', 'sp')), parts along dimension 0, may hold values from -4 to 4
- log_step: float32 [64], P('tp'), may hold values from -6.91 to -2.3
- decay_real: float32 [64, 64], P('tp'), may hold values from -34 to 0, as said below
- freq: float32 [64, 64], P('tp'), may hold values from 0.5 to 8
- in_real: float32 [64, 64, 16], P('tp'), may hold values from -1 to 1
- in_imag: float32 [64, 64, 16], P('tp'), may hold values from -1 to 1
- out_real: float32 [64, 16, 64], P('tp'), may hold values from -0.5 to 0.5
- out_imag: float32 [64, 16, 64], P('tp'), may hold values from -0.5 to 0.5
- skip: float32 [1024], P('tp'), may hold values from -3 to 3
- w_glu: bfloat16 [1024, 1024], replicated, may hold values from -0.1875 to 0.1875
- b_glu: float32 [1024], replicated, may hold values from -3 to 3
- w_branch: bfloat16 [1024, 2048], replicated, may hold values from -0.1875 to 0.1875
- norm_gain: float32 [2048], replicated, may hold values from 0.1 to 1.9
- w_gate: bfloat16 [2048, 5632], P('sp', 'tp'), may hold values from -0.125 to 0.125
- w_up: bfloat16 [2048, 5632], P('sp', 'tp'), may hold values from -0.125 to 0.125
- w_down: bfloat16 [5632, 2048], P('tp', 'sp'), may hold values from -0.078125 to 0.078125
Outputs:
- mixed: bfloat16 [8192, 2048], P(('grp', 'sp', 'tp')), parts along dimension 0
There are 2 independent parts, one for each index of `grp`. A program takes and returns all parts, laid end to end along the dimension named above; an argument that names none is the same for every part. Nothing has to cross between parts.
Inputs may be any that keep to these rules, and one draw needn't show every extreme that they name: `decay_real`: negative in every entry.
All inputs are finite; a program needn't handle non-finite values.
Results may differ from a plain program's by a relative error of at most 0.015.
Values may be sent and summed in bfloat16 or wider, within the bound.
A program may use at most 128 MiB of HBM per device.

v0:
```python
import math
import jax
import jax.numpy as jnp
from jax import lax
from jax.sharding import Mesh
from jax.sharding import PartitionSpec as P

SP = ("sp_0", "sp_1")
GRP_SP = ("grp", "sp_0", "sp_1")
GRP_SP_TP = ("grp", "sp_0", "sp_1", "tp")
EPS = 1e-06


def sent_together(arrays, axis, dim, along):
    ends, at = ([], 0)
    for a in arrays[:-1]:
        at += a.shape[along]
        ends.append(at)
    both = jnp.concatenate(arrays, axis=along)
    return tuple(jnp.split(lax.all_gather(both, axis, axis=dim, tiled=True), ends, axis=along))


def neutral_like(shard, identity):
    return jax.tree.map(
        lambda a, e: jnp.broadcast_to(jnp.asarray(e, a.dtype), a.shape), shard, identity
    )


def all_in_one(shard, axis):
    leaves = jax.tree.leaves(shard)
    turns = sorted(range(len(leaves)), key=lambda k: -leaves[k].size)
    width = (1, *leaves[turns[0]].shape)[-1]
    lines = [
        jnp.pad(leaves[k].reshape(-1), (0, -leaves[k].size % width)).reshape(-1, width)
        for k in turns
    ]
    both, at, found = (lax.all_gather(jnp.concatenate(lines), axis), 0, {})
    for k, line in zip(turns, lines):
        piece = both[:, at : at + len(line)].reshape(len(both), -1)
        found[k] = piece[:, : leaves[k].size].reshape(-1, *leaves[k].shape)
        at += len(line)
    numbers = iter(range(len(leaves)))
    return jax.tree.map(lambda _: found[next(numbers)], shard)


def entering_2(shard, axes, combine, identity):
    before = start = neutral_like(shard, identity)
    so_far = shard
    for axis in reversed(axes):
        count, place = (lax.axis_size(axis), lax.axis_index(axis))
        pieces = all_in_one(so_far, axis)
        inside, so_far = (start, start)
        for k in range(count):
            passed = k < place
            so_far = combine(so_far, jax.tree.map(lambda part: part[k], pieces))
            inside = jax.tree.map(lambda new, old: jnp.where(passed, new, old), so_far, inside)
        before = combine(inside, before)
    return before


def sent_to_all(shard, axis):
    count = lax.axis_size(axis)
    return lax.all_to_all(
        jnp.broadcast_to(shard[None], (count, *shard.shape)), axis, 0, 0, tiled=True
    )


def in_order(pieces, dim):
    dims = list(pieces.shape[1:])
    dims[dim] *= pieces.shape[0]
    return jnp.moveaxis(pieces, 0, dim).reshape(dims)


def gather_directly(shard, axis, dim):
    pieces = sent_to_all(shard, axis)
    return in_order(pieces, dim)


def cut_along(shard, dim, count):
    dims = shard.shape
    pieces = shard.reshape(*dims[:dim], count, dims[dim] // count, *dims[dim + 1 :])
    return jnp.moveaxis(pieces, dim, 0)


def summed_on_arrival(shard, axis, dim):
    pieces = cut_along(shard, dim, lax.axis_size(axis))
    arrived = lax.all_to_all(pieces, axis, split_axis=0, concat_axis=0, tiled=True)
    return arrived.astype(jnp.float32).sum(axis=0)


def discretize(log_step, decay_real, freq, in_real, in_imag):
    step_size = jnp.exp(log_step)[:, None]
    magnitude = jnp.exp(decay_real * step_size)
    abar_re = magnitude * jnp.cos(freq * step_size)
    abar_im = magnitude * jnp.sin(freq * step_size)
    denominator = decay_real * decay_real + freq * freq
    less_re = abar_re - 1.0
    hold_re = ((less_re * decay_real + abar_im * freq) / denominator)[..., None]
    hold_im = ((abar_im * decay_real - less_re * freq) / denominator)[..., None]
    bbar_re = hold_re * in_real - hold_im * in_imag
    bbar_im = hold_re * in_imag + hold_im * in_real
    return (step_size, abar_re, abar_im, bbar_re, bbar_im)


def powers(decay_real, freq, step_size, length):
    steps_up = (jnp.arange(length, dtype=jnp.int32) + 1).astype(jnp.float32)[:, None, None]
    magnitude = jnp.exp((decay_real * step_size)[None] * steps_up)
    phase = (freq * step_size)[None] * steps_up
    return (magnitude * jnp.cos(phase), magnitude * jnp.sin(phase))


def compose(earlier, later):
    a1r, a1i, b1r, b1i = earlier
    a2r, a2i, b2r, b2i = later
    return (
        a2r * a1r - a2i * a1i,
        a2r * a1i + a2i * a1r,
        a2r * b1r - a2i * b1i + b2r,
        a2r * b1i + a2i * b1r + b2i,
    )


def local_states(inputs, decay_real, freq, step_size, bbar_re, bbar_im):
    highest = lax.Precision.DEFAULT
    tok_rows, group_count, unused = inputs.shape
    lanes = group_count * decay_real.shape[1]
    drive_re = jnp.einsum("lgm,gpm->lgp", inputs, bbar_re, precision=highest).reshape(
        tok_rows, lanes
    )
    drive_im = jnp.einsum("lgm,gpm->lgp", inputs, bbar_im, precision=highest).reshape(
        tok_rows, lanes
    )
    span = math.gcd(tok_rows, 16)
    spans = tok_rows // span
    rate = (decay_real * step_size).reshape(lanes)
    turn = (freq * step_size).reshape(lanes)
    later = jnp.arange(span, dtype=jnp.int32)[:, None]
    earlier = jnp.arange(span, dtype=jnp.int32)[None, :]
    lag = (later - earlier).astype(jnp.float32)
    causal = (later >= earlier)[..., None]
    lag_pos = jnp.maximum(lag, 0.0)[..., None]
    table_mag = jnp.exp(rate[None, None] * lag_pos)
    table_re = jnp.where(causal, table_mag * jnp.cos(turn[None, None] * lag_pos), 0.0)
    table_im = jnp.where(causal, table_mag * jnp.sin(turn[None, None] * lag_pos), 0.0)
    block_re = drive_re.reshape(spans, 1, span, lanes)
    block_im = drive_im.reshape(spans, 1, span, lanes)
    inner_re = jnp.sum(table_re[None] * block_re - table_im[None] * block_im, axis=2)
    inner_im = jnp.sum(table_re[None] * block_im + table_im[None] * block_re, axis=2)
    steps_up = (jnp.arange(span, dtype=jnp.int32) + 1).astype(jnp.float32)[:, None]
    pow_mag = jnp.exp(rate[None] * steps_up)
    pow_re = pow_mag * jnp.cos(turn[None] * steps_up)
    pow_im = pow_mag * jnp.sin(turn[None] * steps_up)
    span_re = pow_re[-1]
    span_im = pow_im[-1]

    def carry_step(entering, ends):
        next_re = span_re * entering[0] - span_im * entering[1] + ends[0]
        next_im = span_re * entering[1] + span_im * entering[0] + ends[1]
        return ((next_re, next_im), entering)

    zeros = jnp.zeros((lanes,), jnp.float32)
    unused_carry, entering = lax.scan(
        carry_step, (zeros, zeros), (inner_re[:, -1], inner_im[:, -1])
    )
    state_re = inner_re + pow_re[None] * entering[0][:, None] - pow_im[None] * entering[1][:, None]
    state_im = inner_im + pow_re[None] * entering[1][:, None] + pow_im[None] * entering[0][:, None]
    shape = (tok_rows, group_count, decay_real.shape[1])
    return (state_re.reshape(shape), state_im.reshape(shape))


def readout(state_re, state_im, out_real, out_imag, skip_mat, inputs):
    highest = lax.Precision.DEFAULT
    values = (
        jnp.einsum("lgp,gmp->lgm", state_re, out_real, precision=highest)
        - jnp.einsum("lgp,gmp->lgm", state_im, out_imag, precision=highest)
        + skip_mat[None] * inputs
    )
    values = jax.nn.gelu(values)
    return values.reshape(values.shape[0], -1).astype(jnp.bfloat16)


def row_norm(stream, norm_gain):
    scale_rows = lax.rsqrt(jnp.mean(stream * stream, axis=-1, keepdims=True) + EPS)
    return (stream * scale_rows * norm_gain).astype(jnp.bfloat16)


def per_device(
    ssm_input,
    residual_in,
    log_step,
    decay_real,
    freq,
    in_real,
    in_imag,
    out_real,
    out_imag,
    skip,
    w_glu,
    b_glu,
    w_branch,
    norm_gain,
    w_gate,
    w_up,
    w_down,
):
    tok_rows, width_local = ssm_input.shape
    group_count = log_step.shape[0]
    group_size = in_real.shape[2]
    tp_count = lax.axis_size("tp")
    tp_index = lax.axis_index("tp")
    own_rows = tok_rows // tp_count
    gate_whole, up_whole = sent_together((w_gate, w_up), SP, 0, 1)
    step_size, abar_re, abar_im, bbar_re, bbar_im = discretize(
        log_step, decay_real, freq, in_real, in_imag
    )
    pow_re, pow_im = powers(decay_real, freq, step_size, tok_rows)
    inputs = ssm_input.astype(jnp.float32).reshape(tok_rows, group_count, group_size)
    local_re, local_im = local_states(inputs, decay_real, freq, step_size, bbar_re, bbar_im)
    identity = (
        jnp.ones_like(abar_re),
        jnp.zeros_like(abar_re),
        jnp.zeros_like(abar_re),
        jnp.zeros_like(abar_re),
    )
    carried = entering_2(
        (pow_re[-1], pow_im[-1], local_re[-1], local_im[-1]), SP, compose, identity
    )
    state_re = local_re + pow_re * carried[2][None] - pow_im * carried[3][None]
    state_im = local_im + pow_re * carried[3][None] + pow_im * carried[2][None]
    mixer_out = readout(
        state_re, state_im, out_real, out_imag, skip.reshape(group_count, group_size), inputs
    )
    mixer_rows = lax.all_to_all(mixer_out, "tp", split_axis=0, concat_axis=1, tiled=True)
    glu_pre = jnp.dot(mixer_rows, w_glu, preferred_element_type=jnp.float32) + b_glu
    gated = (mixer_rows.astype(jnp.float32) * jax.nn.sigmoid(glu_pre)).astype(jnp.bfloat16)
    residual_own = lax.dynamic_slice_in_dim(residual_in, tp_index * own_rows, own_rows, 0)
    stream = residual_own.astype(jnp.float32) + jnp.dot(
        gated, w_branch, preferred_element_type=jnp.float32
    )
    normed = row_norm(stream, norm_gain)
    normed_all = gather_directly(normed, "tp", 0)
    gate_sum = jnp.dot(normed_all, gate_whole, preferred_element_type=jnp.float32)
    up_sum = jnp.dot(normed_all, up_whole, preferred_element_type=jnp.float32)
    hidden = (jax.nn.silu(gate_sum) * up_sum).astype(jnp.bfloat16)
    down_whole = lax.all_gather(w_down, SP, axis=1, tiled=True)
    summed = summed_on_arrival(
        jnp.dot(hidden, down_whole, preferred_element_type=jnp.float32).astype(jnp.bfloat16),
        "tp",
        0,
    )
    return (stream + summed).astype(jnp.bfloat16)


def solution(mesh):
    torus = Mesh(
        mesh.devices.reshape(mesh.shape["grp"], 16, 2, mesh.shape["tp"]),
        ("grp", "sp_0", "sp_1", "tp"),
    )
    in_specs = (
        P(GRP_SP, "tp"),
        P(GRP_SP, None),
        P("tp"),
        P("tp", None),
        P("tp", None),
        P("tp", None, None),
        P("tp", None, None),
        P("tp", None, None),
        P("tp", None, None),
        P("tp"),
        P(),
        P(),
        P(),
        P(),
        P(SP, "tp"),
        P(SP, "tp"),
        P("tp", SP),
    )
    out_specs = P(GRP_SP_TP, None)
    return jax.shard_map(
        per_device, mesh=torus, in_specs=in_specs, out_specs=out_specs, check_vma=False
    )
```

profile of v0, /device:TPU:33, one launch (start us, length us, event | category | flops | bytes accessed | tf_op | source)
XLA Modules:
  0.0 209.0 jit_solution(3152876637672829027)
XLA Ops:
  6.6 1.9 pad_maximum_fusion
  8.6 0.7 all-gather.7.cloned.1.call-update
  9.4 0.7 exp.36
  10.0 0.8 fusion.68
  11.0 0.9 copy.43
  12.0 5.8 %fusion.19 = (f32[16,16,1024]{2,1,0:T(8,128)}, f32[16,16,1024]{2,1,0:T(8,128)}) fusion(f32[1024]{0:T(1024)S(1)} %mul.861, f32[16,16]{1,0:T(8,128)S(1)} %convert_maximum_fusion, f32[1024]{0:T(1024)S(1)} %mul.856, pred[16,16]{1,0:T(8,128)(4,1)S(1)} %iota_compare_fusion), kind=kLoop, calls=%fused_computation.33 | loop fusion | flops 1572864 | bytes 2106624 | tf_op jit(solution)/shard_map/jit(_where)/select_n | solution.py:143
  17.8 2.0 convolution_bitcast_fusion.1
  19.8 2.0 convolution_bitcast_fusion
  21.8 1.5 copy.44
  23.4 1.1 mul.878
  24.5 1.5 copy.45
  26.1 1.1 mul.885
  27.2 6.3 %add_reduce_fusion = (f32[8,16,1024]{2,1,0:T(8,128)S(1)}, f32[8,16,1024]{2,1,0:T(8,128)S(1)}) fusion(f32[8,16,1024]{2,1,0:T(8,128)} %mul.885, f32[16,16,1024]{2,1,0:T(8,128)} %get-tuple-element.125, f32[8,16,1024]{2,1,0:T(8,128)} %mul.878, f32[16,16,1024]{2,1,0:T(8,128)} %get-tuple-element.124), kind=kLoop, calls=%fused_computation.6 | loop fusion | flops 16515072 | bytes 4194304 | tf_op jit(solution)/shard_map/reduce_sum | solution.py:148
  33.6 0.3 fusion.55
  34.0 12.5 %while.17 = (s32[]{:T(128)}, f32[1024]{0:T(1024)S(1)}, f32[1024]{0:T(1024)S(1)}, f32[8,1024]{1,0:T(8,128)S(1)}, f32[8,1024]{1,0:T(8,128)}, /*index=5*/f32[1024]{...) while((s32[]{:T(128)}, f32[1024]{0:T(1024)S(1)}, ...), condition=%wide.region_3.4_spmd.clone, body=%wide.region_2.3_spmd.clone.sunk | while | flops 10243 | bytes 90243 | solution.py:162
  34.0 0.1 dynamic_update_slice.11
  34.2 1.4 dynamic_update_slice.12
  35.6 0.1 dynamic_update_slice.11
  35.7 1.4 dynamic_update_slice.12
  37.2 0.1 dynamic_update_slice.11
  37.3 1.4 dynamic_update_slice.12
  38.7 0.1 dynamic_update_slice.11
  38.9 1.4 dynamic_update_slice.12
  40.4 1.4 dynamic_update_slice.12
  42.0 1.4 dynamic_update_slice.12
  43.5 1.4 dynamic_update_slice.12
  45.1 1.4 dynamic_update_slice.12
  46.5 1.9 multiply_add_fusion.1
  48.4 1.3 add.447
  49.8 2.3 %sub.173 = f32[128,16,64]{2,1,0:T(8,128)} reshape(f32[8,16,1024]{2,1,0:T(8,128)} %get-tuple-element.118) | data formatting | bytes 1048576 | tf_op jit(solution)/shard_map/sub | solution.py:165
  52.2 0.7 slice_bitcast_fusion.1
  52.9 3.9 %fusion.22 = (f32[128,16,64]{2,1,0:T(8,128)S(1)}, f32[128,16,64]{2,1,0:T(8,128)S(1)}) fusion(f32[16,64]{1,0:T(8,128)S(1)} %get-tuple-element.133, f32[128]{0:T(128)S(1)} %add_convert_fusion.1, f32[16,64]{1,0:T(8,128)S(1)} %get-tuple-element.132), kind=kLoop, calls=%fused_computation.36 | loop fusion | flops 524288 | bytes 1057280 | tf_op jit(solution)/shard_map/mul | solution.py:109
  56.8 22.0 %all-gather = f32[128,64]{1,0:T(8,128)S(1)} all-gather(f32[64,64]{1,0:T(8,128)S(1)} %pad_maximum_fusion.1), channel_id=2, replica_groups=mesh['grp'=2,'sp_0'=16,'sp_1'=2,'tp'=4] {'sp_1'}, dimensions={0}, use_global_device_ids=true | all-gather | bytes 49152 | tf_op jit(solution)/shard_map/all_gather | solution.py:37
  78.9 31.6 %all-gather.1 = f32[1024,64]{1,0:T(8,128)S(1)} all-gather(f32[64,64]{1,0:T(8,128)S(1)} %pad_maximum_fusion.2), channel_id=3, replica_groups=mesh['grp'=2,'sp_0'=16,'sp_1'=2,'tp'=4] {'sp_0'}, dimensions={0}, use_global_device_ids=true | all-gather | bytes 278528 | tf_op jit(solution)/shard_map/all_gather | solution.py:37
  110.6 6.7 %multiply_add_fusion = (bf16[128,16,64]{2,1,0:T(8,128)(2,1)S(1)}, bf16[128,16,64]{2,1,0:T(8,128)(2,1)S(1)}) fusion(f32[128,16,64]{2,1,0:T(8,128)S(1)} %add.447, f32[16,64]{1,0:T(8,128)S(1)} %add_bitcast_fusion, f32[16,64]{1,0:T(8,128)S(1)} %get-tuple-element.108, f32[16,64]{1,0:T(8,128)S(1)} %get-tuple-element.133, f32[128]{0:T(128)S(1)} %add_convert_fusion.1, ...), kind=kLoop, calls=%fused_computation.42 | loop fusion | flops 1835008 | bytes 1589760 | tf_op jit(solution)/shard_map/add | solution.py:229
  117.3 0.4 fusion.25
  117.7 1.3 fusion.44
  119.0 0.2 convert_element_type.64
  119.2 0.8 copy.48
  120.0 4.2 %all-to-all-start = ((bf16[4,32,256]{2,1,0:T(8,128)(2,1)}), bf16[4,32,256]{2,1,0:T(8,128)(2,1)S(1)}, u32[]{:S(2)}, u32[]{:S(2)}) async-start(bf16[4,32,256]{2,1,0:T(8,128)(2,1)} %copy.48), calls=%async_computation | async-start | bytes 131072 | tf_op jit(solution)/shard_map/all_to_all | solution.py:233
  124.2 4.5 %all-to-all-done = bf16[4,32,256]{2,1,0:T(8,128)(2,1)S(1)} async-done(((bf16[4,32,256]{2,1,0:T(8,128)(2,1)}), bf16[4,32,256]{2,1,0:T(8,128)(2,1)S(1)}, u32[]{:S(2)}, u32[]{:S(2)}) %all-to-all-start) | async-done | bytes 65568 | tf_op jit(solution)/shard_map/all_to_all | solution.py:233
  128.7 3.5 %multiply_reduce_fusion = (f32[32]{0:T(128)S(1)}, f32[32,2048]{1,0:T(8,128)S(1)}) fusion(bf16[1024,2048]{1,0:T(8,128)(2,1)} %param.31, bf16[32,1024]{1,0:T(8,128)(2,1)S(1)} %bitcast.174, bf16[1024,1024]{1,0:T(8,128)(2,1)S(1)} %copy-done, f32[1024]{0:T(1024)S(1)} %copy-done.3, bf16[128,2048]{1,0:T(8,128)(2,1)} %param.20, s32[]{:T(128)S(6)} %select_n.296), kind=kOutput, calls=%fused_computation.57 | convolution fusion | flops 201818080 | bytes 6819972 | tf_op jit(solution)/shard_map/dot_general | solution.py:237
  132.4 9.4 %all_to_all.26 = bf16[4,32,2048]{2,1,0:T(8,128)(2,1)S(1)} all-to-all(bf16[4,32,2048]{2,1,0:T(8,128)(2,1)S(1)} %broadcast_in_dim.32), channel_id=1, replica_groups=mesh['grp'=2,'sp_0'=16,'sp_1'=2,'tp'=4] {'tp'}, dimensions={0} | all-to-all | bytes 1048576 | tf_op jit(solution)/shard_map/all_to_all | solution.py:63
  141.8 4.6 %fusion.2 = f32[128,1408]{1,0:T(8,128)} fusion(bf16[128,2048]{1,0:T(8,128)(2,1)S(1)} %bitcast.167, bf16[2048,2816]{1,0:T(8,128)(2,1)} %all-gather.5.cloned.1.call-done), kind=kOutput, calls=%fused_computation.10 | convolution fusion | flops 738197504 | bytes 7012352 | tf_op jit(solution)/shard_map/dot_general | solution.py:242
  146.3 34.8 %all-gather.7.cloned.1.call-done = bf16[1408,2048]{0,1:T(8,128)(2,1)} async-done(((bf16[1408,64]{0,1:T(8,128)(2,1)}), bf16[1408,2048]{0,1:T(8,128)(2,1)}) %all-gather.7.cloned.1.call-update) | async-done | bytes 5767184 | tf_op jit(solution)/shard_map/all_gather | solution.py:245
  181.1 7.4 %convolution_convert_fusion = bf16[128,2048]{1,0:T(8,128)(2,1)S(1)} fusion(bf16[1408,2048]{0,1:T(8,128)(2,1)} %all-gather.7.cloned.1.call-done, bf16[128,2048]{1,0:T(8,128)(2,1)S(1)} %bitcast.168, bf16[2048,2816]{1,0:T(8,128)(2,1)} %all-gather.5.cloned.1.call-done, f32[128,1408]{1,0:T(8,128)} %fusion.2), kind=kOutput, calls=%fused_computation.14 | convolution fusion | flops 1477738496 | bytes 13303808 | tf_op jit(solution)/shard_map/dot_general | solution.py:247
  188.6 12.9 %all_to_all.27 = bf16[4,32,2048]{2,1,0:T(8,128)(2,1)S(1)} all-to-all(bf16[4,32,2048]{2,1,0:T(8,128)(2,1)S(1)} %bitcast.169), channel_id=1, replica_groups=mesh['grp'=2,'sp_0'=16,'sp_1'=2,'tp'=4] {'tp'}, dimensions={0} | all-to-all | bytes 1048576 | tf_op jit(solution)/shard_map/all_to_all | solution.py:87
  201.5 0.7 add_convert_fusion
  (71 shorter events, 1.5 us)
Async XLA Ops:
  6.5 122.1 %copy-start = (bf16[1024,1024]{1,0:T(8,128)(2,1)S(1)}, bf16[1024,1024]{1,0:T(8,128)(2,1)}, u32[]{:S(2)}) copy-start(bf16[1024,1024]{1,0:T(8,128)(2,1)} %param.29) | copy-start | bytes 6291460
  6.6 135.2 %all-gather.5.cloned.1.call-start = ((), (), s32[]{:S(2)}) async-start(), calls=%async_computation.3 | async-start | bytes 11894784 | tf_op jit(solution)/shard_map/all_gather | solution.py:20
  8.5 172.6 %all-gather.7.cloned.1.call-start = ((), (), s32[]{:S(2)}) async-start(), calls=%async_computation.4 | async-start | bytes 5947392 | tf_op jit(solution)/shard_map/all_gather | solution.py:245
  27.2 24.9 %copy-start.4 = (f32[256]{0:T(256)S(1)}, f32[256]{0:T(256)}, u32[]{:S(2)}) copy-start(f32[256]{0:T(256)} %param.28) | copy-start | bytes 3076
  46.5 70.8 %copy-start.1 = (f32[16,16,64]{2,1,0:T(8,128)S(1)}, f32[16,16,64]{2,1,0:T(8,128)}, u32[]{:S(2)}) copy-start(f32[16,16,64]{2,1,0:T(8,128)} %param.26) | copy-start | bytes 196612
  49.8 78.9 %copy-start.3 = (f32[1024]{0:T(1024)S(1)}, f32[1024]{0:T(1024)}, u32[]{:S(2)}) copy-start(f32[1024]{0:T(1024)} %param.30) | copy-start | bytes 12292
  110.6 21.7 %copy-start.2 = (f32[2048]{0:T(1024)S(1)}, f32[2048]{0:T(1024)}, u32[]{:S(2)}) copy-start(f32[2048]{0:T(1024)} %param.32) | copy-start | bytes 24580
  120.0 8.7 %all-to-all-start = ((bf16[4,32,256]{2,1,0:T(8,128)(2,1)}), bf16[4,32,256]{2,1,0:T(8,128)(2,1)S(1)}, u32[]{:S(2)}, u32[]{:S(2)}) async-start(bf16[4,32,256]{2,1,0:T(8,128)(2,1)} %copy.48), calls=%async_computation | async-start | bytes 131072 | tf_op jit(solution)/shard_map/all_to_all | solution.py:233
Sparse Core Ops, SparseCore 0:
  9.2 101.0 all-gather.4
  112.1 68.9 all-gather.6
where the time goes:
time: 210 us; the launch traced here: 209 us
  blocking collectives  75.9 us (36%)
  waiting for transfers between devices  40.1 us (19%)
  other arithmetic  28.9 us (14%)
  local copies, waits for them, and re-layouts  24.7 us (12%)
  matrix products  21.3 us (10%)
  between operations  13.7 us (7%)
  starting transfers between devices  4.27 us (2%)
    all_gather x2, blocking collectives, all_in_one(): both, at, found = (lax.all_gather(jnp.concatenate(lines), axis), 0, {})  53.6 us
    all_gather x1, waiting for transfers between devices, per_device(): down_whole = lax.all_gather(w_down, SP, axis=1, tiled=True)  34.8 us
    all_to_all x1, blocking collectives, summed_on_arrival(): lax.all_to_all(pieces, axis, split_axis=0, concat_axis=0, tiled=True)  12.9 us
    dynamic_update_slice x16, local copies, waits for them, and re-layouts, local_states(): lax.scan(carry_step, (zeros, zeros), (inner_re[:, -1], inner_im[:, -1]))  12.1 us
    all_to_all x1, blocking collectives, sent_to_all(): lax.all_to_all(jnp.broadcast_to(shard[None], (count, *shard.shape)), axis...  9.36 us
    dot_general x1, matrix products, per_device(): jnp.dot(hidden, down_whole, preferred_element_type=jnp.float32)  7.42 us
    add x1, other arithmetic, per_device(): state_im = local_im + pow_re * carried[3][None] + pow_im * carried[2][None]  6.71 us
    reduce_sum x1, other arithmetic, local_states(): jnp.sum(table_re[None] * block_im + table_im[None] * block_re, axis=2)  6.35 us
  transfers between devices with their start and end apart: 3, of which 2 were waited for; matrix products, arithmetic and copies ran while one was open for 31% of the time, Pallas kernels for 0%

commit v1 on v0

--- a/solution.py
+++ b/solution.py
@@ -242,7 +242,10 @@
     gate_sum = jnp.dot(normed_all, gate_whole, preferred_element_type=jnp.float32)
     up_sum = jnp.dot(normed_all, up_whole, preferred_element_type=jnp.float32)
     hidden = (jax.nn.silu(gate_sum) * up_sum).astype(jnp.bfloat16)
-    down_whole = lax.all_gather(w_down, SP, axis=1, tiled=True)
+    peers = lax.axis_size(SP)
+    parts = jnp.stack([w_down for _ in range(peers)])
+    parts = lax.all_to_all(parts, SP, split_axis=0, concat_axis=0)
+    down_whole = jnp.concatenate(parts, axis=1)
     summed = summed_on_arrival(
         jnp.dot(hidden, down_whole, preferred_element_type=jnp.float32).astype(jnp.bfloat16),
         "tp",

time: 210 us -> 490 us (2.33)
  waiting for transfers between devices: 40.1 us -> 295 us
  starting transfers between devices: 4.27 us -> 19.3 us
  local copies, waits for them, and re-layouts: 24.7 us -> 38.3 us
    all_gather x1, waiting for transfers between devices: 0.01 us -> 230 us  [sent_together(): lax.all_gather(both, axis, axis=dim, tiled=True)]
    all_to_all x0 -> x1, waiting for transfers between devices: none -> 61.5 us  [per_device(): parts = lax.all_to_all(parts, SP, split_axis=0, concat_axis=0)]
    all_gather x1 -> x0, waiting for transfers between devices: 34.8 us -> none  [per_device(): down_whole = lax.all_gather(w_down, SP, axis=1, tiled=True)]
    all_to_all x0 -> x1, starting transfers between devices: none -> 15 us  [per_device(): parts = lax.all_to_all(parts, SP, split_axis=0, concat_axis=0)]
    dynamic_update_slice x16, local copies, waits for them, and re-layouts: 12.1 us -> 22.3 us  [local_states(): lax.scan(carry_step, (zeros, zeros), (inner_re[:, -1], inner_im[:, -1]))]
  transfers between devices with their start and end apart: 3 -> 3, of which waited for: 2 -> 3; matrix products, arithmetic and copies ran while one was open for 31% -> 3% of each run, Pallas kernels for 0% -> 0%
where the time goes in v1:
time: 490 us; the launch traced here: 488 us
  waiting for transfers between devices  295 us (60%)
  blocking collectives  71.4 us (15%)
  local copies, waits for them, and re-layouts  38.3 us (8%)
  other arithmetic  27.8 us (6%)
  matrix products  22.2 us (5%)
  starting transfers between devices  19.3 us (4%)
  between operations  13.7 us (3%)
    all_gather x1, waiting for transfers between devices, sent_together(): lax.all_gather(both, axis, axis=dim, tiled=True)  230 us
    all_to_all x1, waiting for transfers between devices, per_device(): parts = lax.all_to_all(parts, SP, split_axis=0, concat_axis=0)  61.5 us
    all_gather x2, blocking collectives, all_in_one(): both, at, found = (lax.all_gather(jnp.concatenate(lines), axis), 0, {})  49.5 us
    dynamic_update_slice x16, local copies, waits for them, and re-layouts, local_states(): lax.scan(carry_step, (zeros, zeros), (inner_re[:, -1], inner_im[:, -1]))  22.3 us
    all_to_all x1, starting transfers between devices, per_device(): parts = lax.all_to_all(parts, SP, split_axis=0, concat_axis=0)  15 us
    all_to_all x1, blocking collectives, summed_on_arrival(): lax.all_to_all(pieces, axis, split_axis=0, concat_axis=0, tiled=True)  12.5 us
  transfers between devices with their start and end apart: 3, of which 3 were waited for; matrix products, arithmetic and copies ran while one was open for 3% of the time, Pallas kernels for 0%

profile of v1, /device:TPU:33, one launch (start us, length us, event | category | flops | bytes accessed | tf_op | source)
XLA Modules:
  0.0 487.5 jit_solution(12552247322019096665)
XLA Ops:
  6.6 1.1 copy.44
  9.2 2.0 convolution_bitcast_fusion
  11.2 2.0 convolution_bitcast_fusion.1
  13.3 1.5 copy.46
  14.8 1.1 mul.885
  16.1 1.5 copy.45
  17.6 1.1 mul.878
  19.1 4.0 fusion.19
  23.1 6.2 %add_reduce_fusion = (f32[8,16,1024]{2,1,0:T(8,128)S(1)}, f32[8,16,1024]{2,1,0:T(8,128)S(1)}) fusion(f32[8,16,1024]{2,1,0:T(8,128)} %mul.885, f32[16,16,1024]{2,1,0:T(8,128)S(1)} %get-tuple-element.125, f32[8,16,1024]{2,1,0:T(8,128)} %mul.878, f32[16,16,1024]{2,1,0:T(8,128)S(1)} %get-tuple-element.124), kind=kLoop, calls=%fused_computation.6 | loop fusion | flops 16515072 | bytes 4194304 | tf_op jit(solution)/shard_map/reduce_sum | solution.py:148
  29.4 22.7 %while.17 = (s32[]{:T(128)}, f32[1024]{0:T(1024)S(1)}, f32[1024]{0:T(1024)S(1)}, f32[8,1024]{1,0:T(8,128)}, f32[8,1024]{1,0:T(8,128)}, /*index=5*/f32[1024]{0:T(...) while((s32[]{:T(128)}, f32[1024]{0:T(1024)S(1)}, ...), condition=%wide.region_3.4_spmd.clone, body=%wide.region_2.3_spmd.clone.sunk | while | flops 10243 | bytes 90251 | solution.py:162
  29.5 1.4 dynamic_update_slice.11
  30.9 1.4 dynamic_update_slice.12
  32.3 1.4 dynamic_update_slice.11
  33.7 1.4 dynamic_update_slice.12
  35.1 1.4 dynamic_update_slice.11
  36.5 1.4 dynamic_update_slice.12
  38.0 1.4 dynamic_update_slice.11
  39.4 1.4 dynamic_update_slice.12
  40.8 1.4 dynamic_update_slice.11
  42.2 1.4 dynamic_update_slice.12
  43.6 1.4 dynamic_update_slice.11
  45.0 1.4 dynamic_update_slice.12
  46.5 1.4 dynamic_update_slice.11
  47.9 1.4 dynamic_update_slice.12
  49.3 1.4 dynamic_update_slice.11
  50.7 1.4 dynamic_update_slice.12
  52.1 1.9 multiply_add_fusion.1
  54.0 1.3 add.447
  55.3 2.3 sub.173
  58.4 3.9 fusion.22
  62.3 22.0 %all-gather = f32[128,64]{1,0:T(8,128)S(1)} all-gather(f32[64,64]{1,0:T(8,128)S(1)} %pad_maximum_fusion.1), channel_id=2, replica_groups=mesh['grp'=2,'sp_0'=16,'sp_1'=2,'tp'=4] {'sp_1'}, dimensions={0}, use_global_device_ids=true | all-gather | bytes 49152 | tf_op jit(solution)/shard_map/all_gather | solution.py:37
  84.3 27.6 %all-gather.1 = f32[1024,64]{1,0:T(8,128)} all-gather(f32[64,64]{1,0:T(8,128)S(1)} %pad_maximum_fusion.2), channel_id=3, replica_groups=mesh['grp'=2,'sp_0'=16,'sp_1'=2,'tp'=4] {'sp_0'}, dimensions={0}, use_global_device_ids=true | all-gather | bytes 278528 | tf_op jit(solution)/shard_map/all_gather | solution.py:37
  112.0 1.2 add_bitcast_fusion.1
  113.2 6.7 %multiply_add_fusion = (bf16[128,16,64]{2,1,0:T(8,128)(2,1)S(1)}, bf16[128,16,64]{2,1,0:T(8,128)(2,1)S(1)}) fusion(f32[128,16,64]{2,1,0:T(8,128)S(1)} %add.447, f32[16,64]{1,0:T(8,128)S(1)} %add_bitcast_fusion, f32[16,64]{1,0:T(8,128)S(1)} %get-tuple-element.108, f32[16,64]{1,0:T(8,128)S(1)} %get-tuple-element.133, f32[128]{0:T(128)S(1)} %add_convert_fusion.1, ...), kind=kLoop, calls=%fused_computation.42 | loop fusion | flops 1835008 | bytes 1589760 | tf_op jit(solution)/shard_map/add | solution.py:229
  119.9 1.3 fusion.25
  121.2 1.4 fusion.44
  123.5 4.3 all-to-all-start
  127.8 1.7 pad_maximum_fusion
  129.6 2.7 all-to-all-done
  132.3 3.5 multiply_reduce_fusion
  136.0 9.4 %all_to_all.31 = bf16[4,32,2048]{2,1,0:T(8,128)(2,1)S(1)} all-to-all(bf16[4,32,2048]{2,1,0:T(8,128)(2,1)S(1)} %broadcast_in_dim.32), channel_id=1, replica_groups=mesh['grp'=2,'sp_0'=16,'sp_1'=2,'tp'=4] {'tp'}, dimensions={0} | all-to-all | bytes 1048576 | tf_op jit(solution)/shard_map/all_to_all | solution.py:63
  145.4 3.2 stack.2
  148.6 15.0 %all-to-all-start.2 = ((bf16[32,1408,64]{1,2,0:T(8,128)(2,1)}), bf16[32,1408,64]{1,2,0:T(8,128)(2,1)}, u32[]{:S(2)}, u32[]{:S(2)}) async-start(bf16[32,1408,64]{1,2,0:T(8,128)(2,1)} %stack.2), calls=%async_computation.2 | async-start | bytes 11534336 | tf_op jit(solution)/shard_map/all_to_all | solution.py:247
  163.6 230.3 %all-gather.4.cloned.1.call-done = bf16[2048,2816]{1,0:T(8,128)(2,1)} async-done(((bf16[64,2816]{1,0:T(8,128)(2,1)}), bf16[2048,2816]{1,0:T(8,128)(2,1)}) %all-gather.4.cloned.1.call-update) | async-done | bytes 11534352 | tf_op jit(solution)/shard_map/all_gather | solution.py:20
  393.9 4.6 fusion.2
  398.5 61.5 %all-to-all-done.2 = bf16[32,1408,64]{1,2,0:T(8,128)(2,1)} async-done(((bf16[32,1408,64]{1,2,0:T(8,128)(2,1)}), bf16[32,1408,64]{1,2,0:T(8,128)(2,1)}, u32[]{:S(2)}, u32[]{:S(2)}) %all-to-all-start.2) | async-done | bytes 5767200 | tf_op jit(solution)/shard_map/all_to_all | solution.py:247
  460.0 7.4 %convolution_convert_fusion = bf16[128,2048]{1,0:T(8,128)(2,1)S(1)} fusion(bf16[1408,2048]{0,1:T(8,128)(2,1)} %bitcast.25, bf16[128,2048]{1,0:T(8,128)(2,1)S(1)} %bitcast.171, bf16[2048,2816]{1,0:T(8,128)(2,1)} %all-gather.4.cloned.1.call-done, f32[128,1408]{1,0:T(8,128)} %fusion.2), kind=kOutput, calls=%fused_computation.14 | convolution fusion | flops 1477738496 | bytes 13303808 | tf_op jit(solution)/shard_map/dot_general | solution.py:250
  467.4 12.5 %all_to_all.32 = bf16[4,32,2048]{2,1,0:T(8,128)(2,1)S(1)} all-to-all(bf16[4,32,2048]{2,1,0:T(8,128)(2,1)S(1)} %bitcast.172), channel_id=1, replica_groups=mesh['grp'=2,'sp_0'=16,'sp_1'=2,'tp'=4] {'tp'}, dimensions={0} | all-to-all | bytes 1048576 | tf_op jit(solution)/shard_map/all_to_all | solution.py:87
  (73 shorter events, 5.1 us)
Async XLA Ops:
  6.5 125.8 %copy-start = (bf16[1024,1024]{1,0:T(8,128)(2,1)S(1)}, bf16[1024,1024]{1,0:T(8,128)(2,1)}, u32[]{:S(2)}) copy-start(bf16[1024,1024]{1,0:T(8,128)(2,1)} %param.29) | copy-start | bytes 6291460
  29.3 82.6 %copy-start.5 = (f32[256]{0:T(256)S(1)}, f32[256]{0:T(256)}, u32[]{:S(2)}) copy-start(f32[256]{0:T(256)} %param.28) | copy-start | bytes 3076
  55.3 72.5 %copy-start.2 = (bf16[64,1408]{1,0:T(8,128)(2,1)S(1)}, bf16[64,1408]{1,0:T(8,128)(2,1)}, u32[]{:S(2)}) copy-start(bf16[64,1408]{1,0:T(8,128)(2,1)} %param.34) | copy-start | bytes 540676
  57.7 74.6 %copy-start.4 = (f32[1024]{0:T(1024)S(1)}, f32[1024]{0:T(1024)}, u32[]{:S(2)}) copy-start(f32[1024]{0:T(1024)} %param.30) | copy-start | bytes 12292
  119.9 15.9 %copy-start.3 = (f32[2048]{0:T(1024)S(1)}, f32[2048]{0:T(1024)}, u32[]{:S(2)}) copy-start(f32[2048]{0:T(1024)} %param.32) | copy-start | bytes 24580
  121.2 24.2 %copy-start.1 = (bf16[1408,64]{0,1:T(8,128)(2,1)S(1)}, bf16[1408,64]{0,1:T(8,128)(2,1)}, u32[]{:S(2)}) copy-start(bf16[1408,64]{0,1:T(8,128)(2,1)} %param.35) | copy-start | bytes 540676
  123.5 8.8 %all-to-all-start = ((bf16[4,32,256]{2,1,0:T(8,128)(2,1)}), bf16[4,32,256]{2,1,0:T(8,128)(2,1)S(1)}, u32[]{:S(2)}, u32[]{:S(2)}) async-start(bf16[4,32,256]{2,1,0:T(8,128)(2,1)} %copy.49), calls=%async_computation | async-start | bytes 131072 | tf_op jit(solution)/shard_map/all_to_all | solution.py:233
  127.8 266.1 %all-gather.4.cloned.1.call-start = ((), (), s32[]{:S(2)}) async-start(), calls=%async_computation.4 | async-start | bytes 11894784 | tf_op jit(solution)/shard_map/all_gather | solution.py:20
  148.6 311.4 %all-to-all-start.2 = ((bf16[32,1408,64]{1,2,0:T(8,128)(2,1)}), bf16[32,1408,64]{1,2,0:T(8,128)(2,1)}, u32[]{:S(2)}, u32[]{:S(2)}) async-start(bf16[32,1408,64]{1,2,0:T(8,128)(2,1)} %stack.2), calls=%async_computation.2 | async-start | bytes 11534336 | tf_op jit(solution)/shard_map/all_to_all | solution.py:247
Sparse Core Ops, SparseCore 0:
  130.5 263.4 all-gather.3
